TPU v7x, 256 devices: a whole 4x4x8 slice. The times are simulated.
256 devices in a mesh: sp: 32 (over z, x), tp: 8 (over y, core).
Axes of the slice: x: 4, y: 4, z: 8, core: 2. Of those that a mesh axis runs over, the one named last changes fastest.
Arguments:
- broad_probe_tensor: bfloat16 [16384, 1024], P('sp', 'tp'), may hold values from -6 to 6
- broad_lookup_tensor: bfloat16 [16384, 1024], P('sp', 'tp'), may hold values from -6 to 6
- broad_payload_tensor: bfloat16 [16384, 1024], P('sp', 'tp'), may hold values from -6 to 6
- broad_emission_valve: bfloat16 [16384, 1024], P('sp', 'tp'), may hold values from -6 to 6
- slim_probe_tensor: bfloat16 [16384, 1024], P('sp', 'tp'), may hold values from -6 to 6
- slim_lookup_tensor: bfloat16 [16384, 1024], P('sp', 'tp'), may hold values from -6 to 6
- slim_payload_tensor: bfloat16 [16384, 1024], P('sp', 'tp'), may hold values from -6 to 6
- slim_emission_valve: bfloat16 [16384, 1024], P('sp', 'tp'), may hold values from -6 to 6
- broad_forgetting_speed: float32 [8], P('tp'), may hold values from -0.08 to 0
- slim_forgetting_speed: float32 [16], P('tp'), may hold values from -0.08 to 0
- broad_channel_scaling: float32 [1024], P('tp'), may hold values from 0.1 to 1.9
- slim_channel_scaling: float32 [1024], P('tp'), may hold values from 0.1 to 1.9
- surge_forgetting: float32 [16384], P('sp'), may hold values from -2.1 to 0
- broad_emission_proj: bfloat16 [1024, 2048], replicated, may hold values from -0.125 to 0.125
- slim_emission_proj: bfloat16 [1024, 2048], replicated, may hold values from -0.125 to 0.125
- skip_stream: bfloat16 [16384, 2048], P(('sp', 'tp')), may hold values from -6 to 6
- premix_scaling_coeffs: float32 [2048], replicated, may hold values from 0.1 to 1.9
- routed_specialist_ids: int32 [16384, 2], P('sp'), may hold values from 0 to 31, as said below
- routed_specialist_shares: float32 [16384, 2], P('sp'), may hold values from 0.2 to 1
- specialist_valve_proj: bfloat16 [32, 2048, 2048], P('sp', None, 'tp'), may hold values from -0.125 to 0.125
- specialist_expand_proj: bfloat16 [32, 2048, 2048], P('sp', None, 'tp'), may hold values from -0.125 to 0.125
- specialist_contract_proj: bfloat16 [32, 2048, 2048], P('sp', 'tp'), may hold values from -0.125 to 0.125
Outputs:
- result: bfloat16 [16384, 2048], P(('sp', 'tp'))
Inputs may be any that keep to these rules, and one draw needn't show every extreme that they name: `routed_specialist_ids`: each row names two different experts of one group, that is of the same run of 8 consecutive experts. The rows of one device (each aligned block of 64 rows) name each expert at most 8 times, and some expert is named exactly 8 times by the rows of every device.
All inputs are finite; a program needn't handle non-finite values.
Results may differ from a plain program's by a relative error of at most 0.018.
Values may be sent and summed in bfloat16 or wider, within the bound.
A program may use at most 128 MiB of HBM per device.

v0:
```python
import jax
import jax.numpy as jnp
from jax import lax
from jax.sharding import Mesh
from jax.sharding import PartitionSpec as P

BROAD_CHANNEL_DIM = 128
THIN_CHANNEL_DIM = 64
GROUPS = 4
SP = ("sp_0", "sp_1")
SP_TP = ("sp_0", "sp_1", "tp")
rope_base = 10000.0
epsilon = 1e-06


def nothing_yet(value, identity):
    return jax.tree.map(
        lambda part, zero: jnp.zeros_like(part) + jnp.asarray(zero, part.dtype), value, identity
    )


def collected_together(value, axis):
    leaves = jax.tree.leaves(value)
    sequence = sorted(range(len(leaves)), key=lambda k: -leaves[k].size)
    width = (1, *leaves[sequence[0]].shape)[-1]
    lines = [
        jnp.pad(leaves[k].reshape(-1), (0, -leaves[k].size % width)).reshape(-1, width)
        for k in sequence
    ]
    both, at, found = (lax.all_gather(jnp.concatenate(lines), axis), 0, {})
    for k, line in zip(sequence, lines):
        slab = both[:, at : at + len(line)].reshape(len(both), -1)
        found[k] = slab[:, : leaves[k].size].reshape(-1, *leaves[k].shape)
        at += len(line)
    numbers = iter(range(len(leaves)))
    return jax.tree.map(lambda _: found[next(numbers)], value)


def prefix_by_axis(value, axes, combine, identity):
    before = start = nothing_yet(value, identity)
    total = value
    for axis in reversed(axes):
        count, here = (lax.axis_size(axis), lax.axis_index(axis))
        pieces = collected_together(
            jax.tree.map(
                lambda part, kind: part.astype(kind),
                total,
                (jnp.bfloat16, jnp.bfloat16, jnp.bfloat16, jnp.bfloat16),
            ),
            axis,
        )
        inside, total = (start, start)
        for k in range(count):
            passed = k < here
            total = combine(
                total, jax.tree.map(lambda part, own: part[k].astype(own.dtype), pieces, value)
            )
            inside = jax.tree.map(lambda new, old: jnp.where(passed, new, old), total, inside)
        before = combine(inside, before)
    return before


def rotate(payload_tensor, positions):
    channel_dimension = payload_tensor.shape[-1]
    half = channel_dimension // 2
    freq = rope_base ** (-jnp.arange(half, dtype=jnp.float32) * 2.0 / channel_dimension)
    angle = positions.astype(jnp.float32)[:, None, None] * freq[None, None, :]
    cosine = jnp.cos(angle)
    sine = jnp.sin(angle)
    first = payload_tensor[..., :half]
    second = payload_tensor[..., half:]
    return jnp.concatenate([first * cosine - second * sine, first * sine + second * cosine], -1)


def segment_terms(probe_tensor, lookup_tensor, payload_tensor, surge_forgetting, forgetting_speed):
    length = probe_tensor.shape[0]
    segment_tally = jnp.arange(length, dtype=jnp.float32)
    memory_matrix = (
        forgetting_speed[None, :] * segment_tally[:, None] + jnp.cumsum(surge_forgetting)[:, None]
    )
    causal = (segment_tally[:, None] >= segment_tally[None, :])[None]
    level_t = jnp.transpose(memory_matrix)
    gap = level_t[:, :, None] - level_t[:, None, :]
    decay = jnp.where(causal, jnp.exp(jnp.where(causal, gap, 0.0)), 0.0)
    attention_scores = jnp.einsum(
        "szr,yzr->zsy", probe_tensor, lookup_tensor, preferred_element_type=jnp.float32
    )
    weights = (attention_scores * decay).astype(jnp.bfloat16)
    inner = jnp.einsum("htm,mhe->the", weights, payload_tensor, preferred_element_type=jnp.float32)
    factor = jnp.exp(memory_matrix + forgetting_speed[None, :])
    tail = jnp.exp(memory_matrix[-1:, :] - memory_matrix)
    weighted_output = (lookup_tensor.astype(jnp.float32) * tail[:, :, None]).astype(jnp.bfloat16)
    state_update = jnp.einsum(
        "oup,our->upr", weighted_output, payload_tensor, preferred_element_type=jnp.float32
    )
    total = jnp.exp(memory_matrix[-1] + forgetting_speed)
    return (inner, factor, state_update, total)


def read_state(probe_tensor, state):
    return jnp.einsum("thd,hde->the", probe_tensor.astype(jnp.float32), state)


def keeping_multiplier(
    probe_source,
    lookup_tensor,
    payload_tensor,
    forgetting_speed,
    surge_forgetting,
    channel_dimension,
    segment_begin,
):
    length = probe_source.shape[0]
    heads = probe_source.shape[1] // channel_dimension
    places = segment_begin + jnp.arange(length, dtype=jnp.int32)
    spun_probe = rotate(
        probe_source.astype(jnp.float32).reshape(length, heads, channel_dimension), places
    ).astype(jnp.bfloat16)
    spun_lookup = (
        rotate(lookup_tensor.astype(jnp.float32).reshape(length, heads, channel_dimension), places)
        * channel_dimension ** (-0.5)
    ).astype(jnp.bfloat16)
    regrouped_payload = payload_tensor.reshape(length, heads, channel_dimension)
    block = min(512, length)
    count = length // block

    def divider_mark(array):
        return array.reshape((count, block) + array.shape[1:])

    def segment_walker(carry, piece):
        state, prefix = carry
        block_q, block_k, block_v, block_b = piece
        inner, factor, state_update, total = segment_terms(
            block_q, block_k, block_v, block_b, forgetting_speed
        )
        local = inner + factor[:, :, None] * read_state(block_q, state)
        return (
            (total[:, None, None] * state + state_update, prefix * total),
            (local, factor * prefix[None, :]),
        )

    opening_location = (
        jnp.zeros((heads, channel_dimension, channel_dimension), jnp.float32),
        jnp.ones((heads,), jnp.float32),
    )
    (state, decay), (local, reach) = lax.scan(
        segment_walker,
        opening_location,
        (
            divider_mark(spun_probe),
            divider_mark(spun_lookup),
            divider_mark(regrouped_payload),
            divider_mark(surge_forgetting),
        ),
    )
    return (
        spun_probe,
        local.reshape(length, heads, channel_dimension),
        reach.reshape(length, heads),
        decay,
        state,
    )


def finish(sublayer_final, emission_valve, scaling_coefficients):
    length, heads, channel_dimension = sublayer_final.shape
    normed = sublayer_final * lax.rsqrt(
        jnp.mean(sublayer_final * sublayer_final, -1, keepdims=True) + epsilon
    )
    gated = (
        normed.reshape(length, heads * channel_dimension)
        * scaling_coefficients[None, :]
        * jax.nn.silu(emission_valve.astype(jnp.float32))
    )
    return gated.astype(jnp.bfloat16)


def chain(earlier, later):
    return (
        earlier[0] * later[0],
        later[0][:, None, None] * earlier[1] + later[1],
        earlier[2] * later[2],
        later[2][:, None, None] * earlier[3] + later[3],
    )


def slot_positions(chosen, experts, cap):
    listed = chosen.reshape(-1)
    matches = (listed[:, None] == jnp.arange(experts, dtype=jnp.int32)[None, :]).astype(jnp.int32)
    before = jnp.cumsum(matches, 0) - matches
    order = jnp.sum(before * matches, 1)
    return (listed * cap + order).reshape(chosen.shape)


def fill_slots(rows_in, chosen, experts, cap):
    count = rows_in.shape[0]
    places = slot_positions(chosen, experts, cap).reshape(-1)
    owners = jnp.repeat(jnp.arange(count, dtype=jnp.int32), 2)
    source = jnp.full((experts * cap,), count, jnp.int32).at[places].set(owners)
    padded = jnp.concatenate([rows_in, jnp.zeros((1, rows_in.shape[1]), rows_in.dtype)], 0)
    return padded[source].reshape(experts, cap, rows_in.shape[1])


def on_device(
    broad_probe_tensor,
    broad_lookup_tensor,
    broad_payload_tensor,
    broad_emission_valve,
    slim_probe_tensor,
    slim_lookup_tensor,
    slim_payload_tensor,
    slim_emission_valve,
    broad_forgetting_speed,
    slim_forgetting_speed,
    broad_channel_scaling,
    slim_channel_scaling,
    surge_forgetting,
    broad_emission_proj,
    slim_emission_proj,
    skip_stream,
    premix_scaling_coeffs,
    routed_specialist_ids,
    routed_specialist_shares,
    specialist_valve_proj,
    specialist_expand_proj,
    specialist_contract_proj,
):
    length = broad_probe_tensor.shape[0]
    segment_begin = lax.axis_index(SP) * length
    wide_result = keeping_multiplier(
        broad_probe_tensor,
        broad_lookup_tensor,
        broad_payload_tensor,
        broad_forgetting_speed,
        surge_forgetting,
        BROAD_CHANNEL_DIM,
        segment_begin,
    )
    narrow_result = keeping_multiplier(
        slim_probe_tensor,
        slim_lookup_tensor,
        slim_payload_tensor,
        slim_forgetting_speed,
        surge_forgetting,
        THIN_CHANNEL_DIM,
        segment_begin,
    )
    identity = (
        jnp.ones_like(wide_result[3]),
        jnp.zeros_like(wide_result[4]),
        jnp.ones_like(narrow_result[3]),
        jnp.zeros_like(narrow_result[4]),
    )
    incoming = prefix_by_axis(
        (wide_result[3], wide_result[4], narrow_result[3], narrow_result[4]), SP, chain, identity
    )
    mixed_wide = finish(
        wide_result[1] + wide_result[2][:, :, None] * read_state(wide_result[0], incoming[1]),
        broad_emission_valve,
        broad_channel_scaling,
    )
    mixed_narrow = finish(
        narrow_result[1] + narrow_result[2][:, :, None] * read_state(narrow_result[0], incoming[3]),
        slim_emission_valve,
        slim_channel_scaling,
    )
    rows_wide, rows_narrow = (
        lax.all_to_all(mixed_wide, "tp", split_axis=0, concat_axis=1, tiled=True),
        lax.all_to_all(mixed_narrow, "tp", split_axis=0, concat_axis=1, tiled=True),
    )
    projected = jnp.dot(rows_wide, broad_emission_proj, preferred_element_type=jnp.float32)
    projected = projected + jnp.dot(
        rows_narrow, slim_emission_proj, preferred_element_type=jnp.float32
    )
    updated = skip_stream.astype(jnp.float32) + projected
    scale = lax.rsqrt(jnp.mean(updated * updated, -1, keepdims=True) + epsilon)
    normed = (updated * scale * premix_scaling_coeffs[None, :]).astype(jnp.bfloat16)
    rows = normed.shape[0]
    width = normed.shape[1]
    experts = lax.axis_size(SP) * specialist_valve_proj.shape[0]
    cap = rows * GROUPS // experts
    own_ids = lax.dynamic_slice_in_dim(routed_specialist_ids, lax.axis_index("tp") * rows, rows, 0)
    own_weights = lax.dynamic_slice_in_dim(
        routed_specialist_shares, lax.axis_index("tp") * rows, rows, 0
    )
    own_places = slot_positions(own_ids, experts, cap)
    sent = lax.all_to_all(
        fill_slots(normed, own_ids, experts, cap), SP, split_axis=0, concat_axis=0, tiled=True
    )
    arrived = lax.all_gather(sent, "tp", axis=0, tiled=True)
    slots = arrived.reshape(-1, width)
    emission_valve = jnp.dot(slots, specialist_valve_proj[0], preferred_element_type=jnp.float32)
    up = jnp.dot(slots, specialist_expand_proj[0], preferred_element_type=jnp.float32)
    hidden = (jax.nn.silu(emission_valve) * up).astype(jnp.bfloat16)
    summed = lax.psum_scatter(
        jnp.dot(hidden, specialist_contract_proj[0], preferred_element_type=jnp.float32).astype(
            jnp.bfloat16
        ),
        "tp",
        scatter_dimension=0,
        tiled=True,
    )
    expert_out = summed.reshape(experts, cap, width)
    returned = lax.all_to_all(expert_out, SP, split_axis=0, concat_axis=0, tiled=True)
    picked = returned.reshape(experts * cap, width)[own_places]
    mixture = jnp.sum(own_weights[:, :, None] * picked.astype(jnp.float32), 1)
    return (updated + mixture).astype(jnp.bfloat16)


def solution(mesh):
    finer = Mesh(mesh.devices.reshape(8, 4, mesh.shape["tp"]), ("sp_0", "sp_1", "tp"))
    return jax.shard_map(
        on_device,
        mesh=finer,
        in_specs=(
            P(SP, "tp"),
            P(SP, "tp"),
            P(SP, "tp"),
            P(SP, "tp"),
            P(SP, "tp"),
            P(SP, "tp"),
            P(SP, "tp"),
            P(SP, "tp"),
            P("tp"),
            P("tp"),
            P("tp"),
            P("tp"),
            P(SP),
            P(),
            P(),
            P(SP_TP, None),
            P(),
            P(SP, None),
            P(SP, None),
            P(SP, None, "tp"),
            P(SP, None, "tp"),
            P(SP, "tp", None),
        ),
        out_specs=P(SP_TP, None),
        check_vma=False,
    )
```

profile of v0, /device:TPU:2, one launch (start us, length us, event | category | flops | bytes accessed | tf_op | source)
XLA Modules:
  0.0 307.2 jit_solution(5164450144786927147)
XLA Ops:
  6.6 1.1 reduce-window.9
  7.9 0.7 multiply_add_fusion.2
  8.9 0.7 add_exponential_fusion
  9.6 0.7 broadcast_multiply_fusion.2
  10.3 1.0 copy.137
  11.4 1.0 copy.146
  12.4 1.0 copy.138
  16.1 1.3 fusion.80
  18.0 12.2 %all-gather.2 = bf16[4,194,128]{2,1,0:T(8,128)(2,1)S(1)} all-gather(bf16[1,194,128]{2,1,0:T(8,128)(2,1)S(1)} %maximum_bitcast_fusion), channel_id=2, replica_groups=mesh['sp_0'=8,'sp_1'=4,'tp'=8] {'sp_1'}, dimensions={0}, use_global_device_ids=true | all-gather | bytes 248320 | tf_op jit(solution)/shard_map/all_gather | solution.py:30
  34.9 28.8 %all-gather.3 = bf16[8,194,128]{2,1,0:T(8,128)(2,1)S(1)} all-gather(bf16[1,194,128]{2,1,0:T(8,128)(2,1)S(1)} %maximum_bitcast_fusion.1), channel_id=3, replica_groups=mesh['sp_0'=8,'sp_1'=4,'tp'=8] {'sp_0'}, dimensions={0}, use_global_device_ids=true | all-gather | bytes 446976 | tf_op jit(solution)/shard_map/all_gather | solution.py:30
  71.4 0.8 fusion.71
  72.2 4.5 %all-to-all-start = ((bf16[8,64,128]{2,1,0:T(8,128)(2,1)}), bf16[8,64,128]{2,1,0:T(8,128)(2,1)S(1)}, u32[]{:S(2)}, u32[]{:S(2)}) async-start(bf16[8,64,128]{2,1,0:T(8,128)(2,1)} %bitcast.66), calls=%async_computation | async-start | bytes 262144 | tf_op jit(solution)/shard_map/all_to_all | solution.py:268
  79.1 1.1 fusion.21
  80.9 0.8 constant_dynamic-slice_fusion
  82.8 1.0 scatter_custom_fusion
  83.8 0.7 fusion.70
  84.6 4.8 %all-to-all-start.1 = ((bf16[8,64,128]{2,1,0:T(8,128)(2,1)}), bf16[8,64,128]{2,1,0:T(8,128)(2,1)S(1)}, u32[]{:S(2)}, u32[]{:S(2)}) async-start(bf16[8,64,128]{2,1,0:T(8,128)(2,1)} %bitcast.82), calls=%async_computation.1 | async-start | bytes 262144 | tf_op jit(solution)/shard_map/all_to_all | solution.py:269
  89.4 3.1 fusion.74
  92.5 3.0 all-to-all-done.1
  95.5 3.2 %multiply_reduce_fusion.1 = (f32[64]{0:T(128)S(1)}, f32[64,2048]{1,0:T(8,128)S(1)}) fusion(f32[64,2048]{1,0:T(8,128)S(1)} %fusion.74, bf16[1024,2048]{1,0:T(8,128)(2,1)} %param.36, bf16[64,2048]{1,0:T(8,128)(2,1)S(1)} %copy-done.1, bf16[8,64,128]{2,1,0:T(8,128)(2,1)S(1)} %all-to-all-done.1), kind=kOutput, calls=%fused_computation.51 | convolution fusion | flops 269090752 | bytes 5636352 | tf_op jit(solution)/shard_map/dot_general | solution.py:272
  98.9 1.4 gather_fusion
  100.2 35.5 %all_to_all.48 = bf16[32,8,2048]{2,1,0:T(8,128)(2,1)} all-to-all(bf16[32,8,2048]{2,1,0:T(8,128)(2,1)S(1)} %bitcast.268), channel_id=1, replica_groups=mesh['sp_0'=8,'sp_1'=4,'tp'=8] {'sp_0','sp_1'}, dimensions={0} | all-to-all | bytes 2097152 | tf_op jit(solution)/shard_map/all_to_all | solution.py:287
  136.0 47.0 %all-gather.6.cloned.1.call-done = bf16[256,8,2048]{2,1,0:T(8,128)(2,1)} async-done(((bf16[32,8,2048]{2,1,0:T(8,128)(2,1)}), bf16[256,8,2048]{2,1,0:T(8,128)(2,1)}) %all-gather.6.cloned.1.call-update) | async-done | bytes 8388624 | tf_op jit(solution)/shard_map/all_gather | solution.py:290
  183.0 7.3 %fusion.2 = f32[2048,256]{1,0:T(8,128)} fusion(bf16[256,8,2048]{2,1,0:T(8,128)(2,1)} %all-gather.6.cloned.1.call-done, bf16[1,2048,256]{2,1,0:T(8,128)(2,1)} %param.41), kind=kOutput, calls=%fused_computation.5 | convolution fusion | flops 2147483648 | bytes 11534336 | tf_op jit(solution)/shard_map/dot_general | solution.py:292
  190.3 13.1 %convolution_convert_fusion = bf16[2048,2048]{1,0:T(8,128)(2,1)} fusion(bf16[256,8,2048]{2,1,0:T(8,128)(2,1)} %all-gather.6.cloned.1.call-done, f32[2048,256]{1,0:T(8,128)} %fusion.2, bf16[1,256,2048]{2,1,0:T(8,128)(2,1)S(1)} %copy-done, bf16[1,2048,256]{2,1,0:T(8,128)(2,1)S(1)} %copy-done.10), kind=kOutput, calls=%fused_computation.7 | convolution fusion | flops 4302307328 | bytes 20971520 | tf_op jit(solution)/shard_map/dot_general | solution.py:296
  203.4 55.4 %reduce-scatter.2.cloned.1.call-done = bf16[256,2048]{1,0:T(8,128)(2,1)} async-done(((bf16[2048,2048]{1,0:T(8,128)(2,1)}), bf16[256,2048]{1,0:T(8,128)(2,1)}) %reduce-scatter.2.cloned.1.call-update) | async-done | bytes 1048592 | tf_op jit(solution)/shard_map/reduce_scatter | solution.py:295
  258.8 10.1 %all-to-all-start.3 = ((bf16[32,8,2048]{2,1,0:T(8,128)(2,1)}), bf16[32,8,2048]{2,1,0:T(8,128)(2,1)S(1)}, u32[]{:S(2)}, u32[]{:S(2)}) async-start(bf16[32,8,2048]{2,1,0:T(8,128)(2,1)} %bitcast.269), calls=%async_computation.4 | async-start | bytes 2097152 | tf_op jit(solution)/shard_map/all_to_all | solution.py:304
  269.1 0.8 constant_dynamic-slice_fusion.1
  270.0 26.5 %all-to-all-done.3 = bf16[32,8,2048]{2,1,0:T(8,128)(2,1)S(1)} async-done(((bf16[32,8,2048]{2,1,0:T(8,128)(2,1)}), bf16[32,8,2048]{2,1,0:T(8,128)(2,1)S(1)}, u32[]{:S(2)}, u32[]{:S(2)}) %all-to-all-start.3) | async-done | bytes 1048608 | tf_op jit(solution)/shard_map/all_to_all | solution.py:304
  296.5 0.9 gather_fusion.1
  298.1 1.5 multiply_reduce_fusion
  299.6 0.8 add_convert_fusion
  (133 shorter events, 11.1 us)
Async XLA Ops:
  6.5 183.8 %copy-start = (bf16[1,256,2048]{2,1,0:T(8,128)(2,1)S(1)}, bf16[1,256,2048]{2,1,0:T(8,128)(2,1)}, u32[]{:S(2)}) copy-start(bf16[1,256,2048]{2,1,0:T(8,128)(2,1)} %param.43) | copy-start | bytes 3145732
  6.5 9.5 %copy-start.5 = (bf16[512,128]{1,0:T(8,128)(2,1)S(1)}, bf16[512,128]{1,0:T(8,128)(2,1)}, u32[]{:S(2)}) copy-start(bf16[512,128]{1,0:T(8,128)(2,1)} %param.22) | copy-start | bytes 393220
  6.5 9.5 %copy-start.4 = (bf16[512,128]{1,0:T(8,128)(2,1)S(1)}, bf16[512,128]{1,0:T(8,128)(2,1)}, u32[]{:S(2)}) copy-start(bf16[512,128]{1,0:T(8,128)(2,1)} %param.23) | copy-start | bytes 393220
  13.8 3.8 %copy-start.11 = (bf16[512,128]{1,0:T(8,128)(2,1)S(1)}, bf16[512,128]{1,0:T(8,128)(2,1)}, u32[]{:S(2)}) copy-start(bf16[512,128]{1,0:T(8,128)(2,1)} %param.24) | copy-start | bytes 393220
  70.1 1.3 copy-start.2
  70.1 1.3 copy-start.8
  70.7 6.1 %copy-start.7 = (f32[2]{0:T(128)S(1)}, f32[2]{0:T(128)}, u32[]{:S(2)}) copy-start(f32[2]{0:T(128)} %param.31) | copy-start | bytes 28
  72.2 12.4 %all-to-all-start = ((bf16[8,64,128]{2,1,0:T(8,128)(2,1)}), bf16[8,64,128]{2,1,0:T(8,128)(2,1)S(1)}, u32[]{:S(2)}, u32[]{:S(2)}) async-start(bf16[8,64,128]{2,1,0:T(8,128)(2,1)} %bitcast.66), calls=%async_computation | async-start | bytes 262144 | tf_op jit(solution)/shard_map/all_to_all | solution.py:268
  80.2 3.6 %copy-start.3 = (bf16[512,128]{1,0:T(8,128)(2,1)S(1)}, bf16[512,128]{1,0:T(8,128)(2,1)}, u32[]{:S(2)}) copy-start(bf16[512,128]{1,0:T(8,128)(2,1)} %param.29) | copy-start | bytes 393220
  80.2 3.6 %copy-start.9 = (f32[128]{0:T(128)S(1)}, f32[128]{0:T(128)}, u32[]{:S(2)}) copy-start(f32[128]{0:T(128)} %param.33) | copy-start | bytes 1540
  84.6 10.9 %all-to-all-start.1 = ((bf16[8,64,128]{2,1,0:T(8,128)(2,1)}), bf16[8,64,128]{2,1,0:T(8,128)(2,1)S(1)}, u32[]{:S(2)}, u32[]{:S(2)}) async-start(bf16[8,64,128]{2,1,0:T(8,128)(2,1)} %bitcast.82), calls=%async_computation.1 | async-start | bytes 262144 | tf_op jit(solution)/shard_map/all_to_all | solution.py:269
  89.4 6.1 %copy-start.1 = (bf16[64,2048]{1,0:T(8,128)(2,1)S(1)}, bf16[64,2048]{1,0:T(8,128)(2,1)}, u32[]{:S(2)}) copy-start(bf16[64,2048]{1,0:T(8,128)(2,1)} %param.37) | copy-start | bytes 786436
  89.4 93.6 %all-gather.6.cloned.1.call-start = ((), (), s32[]{:S(2)}) async-start(), calls=%async_computation.5 | async-start | bytes 9437184 | tf_op jit(solution)/shard_map/all_gather | solution.py:290
  92.5 6.2 %copy-start.6 = (f32[2048]{0:T(1024)S(1)}, f32[2048]{0:T(1024)}, u32[]{:S(2)}) copy-start(f32[2048]{0:T(1024)} %param.38) | copy-start | bytes 24580
  135.7 54.6 %copy-start.10 = (bf16[1,2048,256]{2,1,0:T(8,128)(2,1)S(1)}, bf16[1,2048,256]{2,1,0:T(8,128)(2,1)}, u32[]{:S(2)}) copy-start(bf16[1,2048,256]{2,1,0:T(8,128)(2,1)} %param.42) | copy-start | bytes 3145732
  135.8 123.1 %reduce-scatter.2.cloned.1.call-start = ((), (), s32[]{:S(2)}) async-start(), calls=%async_computation.6 | async-start | bytes 9437184 | tf_op jit(solution)/shard_map/reduce_scatter | solution.py:295
  258.8 37.6 %all-to-all-start.3 = ((bf16[32,8,2048]{2,1,0:T(8,128)(2,1)}), bf16[32,8,2048]{2,1,0:T(8,128)(2,1)S(1)}, u32[]{:S(2)}, u32[]{:S(2)}) async-start(bf16[32,8,2048]{2,1,0:T(8,128)(2,1)} %bitcast.269), calls=%async_computation.4 | async-start | bytes 2097152 | tf_op jit(solution)/shard_map/all_to_all | solution.py:304
Sparse Core Ops, SparseCore 0:
  135.9 47.0 all-gather.5
  203.6 55.2 reduce-scatter.1
where the time goes:
time: 308 us; the launch traced here: 307 us
  waiting for transfers between devices  132 us (43%)
  blocking collectives  76.5 us (25%)
  matrix products  30.1 us (10%)
  between operations  24.4 us (8%)
  starting transfers between devices  19.7 us (6%)
  local copies, waits for them, and re-layouts  14.4 us (5%)
  other arithmetic  10.2 us (3%)
    reduce_scatter x1, waiting for transfers between devices, on_device(): lax.psum_scatter(jnp.dot(hidden, specialist_contract_proj[0], preferred_e...  55.4 us
    all_gather x1, waiting for transfers between devices, on_device(): arrived = lax.all_gather(sent, 'tp', axis=0, tiled=True)  47 us
    all_gather x2, blocking collectives, collected_together(): both, at, found = (lax.all_gather(jnp.concatenate(lines), axis), 0, {})  41 us
    all_to_all x1, blocking collectives, on_device(): lax.all_to_all(fill_slots(normed, own_ids, experts, cap), SP, split_axis=...  35.5 us
    all_to_all x1, waiting for transfers between devices, on_device(): lax.all_to_all(expert_out, SP, split_axis=0, concat_axis=0, tiled=True)  26.5 us
    dot_general x1, matrix products, on_device(): jnp.dot(hidden, specialist_contract_proj[0], preferred_element_type=jnp.f...  13.1 us
    all_to_all x1, starting transfers between devices, on_device(): lax.all_to_all(expert_out, SP, split_axis=0, concat_axis=0, tiled=True)  10.1 us
    dot_general x1, matrix products, on_device(): jnp.dot(slots, specialist_valve_proj[0], preferred_element_type=jnp.float32)  7.3 us
  transfers between devices with their start and end apart: 5, of which 4 were waited for; matrix products, arithmetic and copies ran while one was open for 4% of the time, Pallas kernels for 0%

commit v1 on v0

--- a/solution.py
+++ b/solution.py
@@ -287,7 +287,9 @@
     sent = lax.all_to_all(
         fill_slots(normed, own_ids, experts, cap), SP, split_axis=0, concat_axis=0, tiled=True
     )
-    arrived = lax.all_gather(sent, "tp", axis=0, tiled=True)
+    arrived = jnp.concatenate(
+        lax.all_to_all(jnp.stack([sent] * lax.axis_size("tp")), "tp", 0, 0), axis=0
+    )
     slots = arrived.reshape(-1, width)
     emission_valve = jnp.dot(slots, specialist_valve_proj[0], preferred_element_type=jnp.float32)
     up = jnp.dot(slots, specialist_expand_proj[0], preferred_element_type=jnp.float32)

time: 308 us -> 357 us (1.16)
  blocking collectives: 76.5 us -> 174 us
  waiting for transfers between devices: 132 us -> 80.1 us
  local copies, waits for them, and re-layouts: 14.4 us -> 18.6 us
    all_to_all x0 -> x1, blocking collectives: none -> 97.3 us  [on_device(): lax.all_to_all(jnp.stack([sent] * lax.axis_size('tp')), 'tp', 0, 0)]
    all_gather x1 -> x0, waiting for transfers between devices: 47 us -> none  [on_device(): arrived = lax.all_gather(sent, 'tp', axis=0, tiled=True)]
    reduce_scatter x1, waiting for transfers between devices: 55.4 us -> 50.6 us  [on_device(): lax.psum_scatter(jnp.dot(hidden, specialist_contract_proj[0], preferred_e...]
    dot_general x1, matrix products: 13.1 us -> 16.8 us  [on_device(): jnp.dot(hidden, specialist_contract_proj[0], preferred_element_type=jnp.f...]
  transfers between devices with their start and end apart: 5 -> 4, of which waited for: 4 -> 3; matrix products, arithmetic and copies ran while one was open for 4% -> 3% of each run, Pallas kernels for 0% -> 0%
where the time goes in v1:
time: 357 us; the launch traced here: 356 us
  blocking collectives  174 us (49%)
  waiting for transfers between devices  80.1 us (22%)
  matrix products  30.2 us (8%)
  between operations  24.1 us (7%)
  starting transfers between devices  19.5 us (5%)
  local copies, waits for them, and re-layouts  18.6 us (5%)
  other arithmetic  10.2 us (3%)
    all_to_all x1, blocking collectives, on_device(): lax.all_to_all(jnp.stack([sent] * lax.axis_size('tp')), 'tp', 0, 0)  97.3 us
    reduce_scatter x1, waiting for transfers between devices, on_device(): lax.psum_scatter(jnp.dot(hidden, specialist_contract_proj[0], preferred_e...  50.6 us
    all_gather x2, blocking collectives, collected_together(): both, at, found = (lax.all_gather(jnp.concatenate(lines), axis), 0, {})  41 us
    all_to_all x1, blocking collectives, on_device(): lax.all_to_all(fill_slots(normed, own_ids, experts, cap), SP, split_axis=...  35.4 us
    all_to_all x1, waiting for transfers between devices, on_device(): lax.all_to_all(expert_out, SP, split_axis=0, concat_axis=0, tiled=True)  26.5 us
    dot_general x1, matrix products, on_device(): jnp.dot(hidden, specialist_contract_proj[0], preferred_element_type=jnp.f...  16.8 us
    all_to_all x1, starting transfers between devices, on_device(): lax.all_to_all(expert_out, SP, split_axis=0, concat_axis=0, tiled=True)  10.1 us
  transfers between devices with their start and end apart: 4, of which 3 were waited for; matrix products, arithmetic and copies ran while one was open for 3% of the time, Pallas kernels for 0%

profile of v1, /device:TPU:2, one launch (start us, length us, event | category | flops | bytes accessed | tf_op | source)
XLA Modules:
  0.0 356.4 jit_solution(7474743858232897169)
XLA Ops:
  6.6 1.1 reduce-window.9
  8.9 0.7 add_exponential_fusion
  10.3 1.0 copy.137
  11.4 1.0 copy.146
  12.4 1.0 copy.138
  16.0 1.3 fusion.70
  17.9 12.2 %all-gather.2 = bf16[4,194,128]{2,1,0:T(8,128)(2,1)S(1)} all-gather(bf16[1,194,128]{2,1,0:T(8,128)(2,1)S(1)} %maximum_bitcast_fusion), channel_id=2, replica_groups=mesh['sp_0'=8,'sp_1'=4,'tp'=8] {'sp_1'}, dimensions={0}, use_global_device_ids=true | all-gather | bytes 248320 | tf_op jit(solution)/shard_map/all_gather | solution.py:30
  34.6 28.8 %all-gather.3 = bf16[8,194,128]{2,1,0:T(8,128)(2,1)S(1)} all-gather(bf16[1,194,128]{2,1,0:T(8,128)(2,1)S(1)} %maximum_bitcast_fusion.1), channel_id=3, replica_groups=mesh['sp_0'=8,'sp_1'=4,'tp'=8] {'sp_0'}, dimensions={0}, use_global_device_ids=true | all-gather | bytes 446976 | tf_op jit(solution)/shard_map/all_gather | solution.py:30
  71.0 0.8 fusion.61
  71.8 4.5 %all-to-all-start = ((bf16[8,64,128]{2,1,0:T(8,128)(2,1)}), bf16[8,64,128]{2,1,0:T(8,128)(2,1)S(1)}, u32[]{:S(2)}, u32[]{:S(2)}) async-start(bf16[8,64,128]{2,1,0:T(8,128)(2,1)} %bitcast.66), calls=%async_computation | async-start | bytes 262144 | tf_op jit(solution)/shard_map/all_to_all | solution.py:268
  78.6 1.1 fusion.10
  80.5 0.8 constant_dynamic-slice_fusion
  82.4 1.0 scatter_custom_fusion
  83.4 0.7 fusion.60
  84.2 4.8 %all-to-all-start.1 = ((bf16[8,64,128]{2,1,0:T(8,128)(2,1)}), bf16[8,64,128]{2,1,0:T(8,128)(2,1)S(1)}, u32[]{:S(2)}, u32[]{:S(2)}) async-start(bf16[8,64,128]{2,1,0:T(8,128)(2,1)} %bitcast.82), calls=%async_computation.1 | async-start | bytes 262144 | tf_op jit(solution)/shard_map/all_to_all | solution.py:269
  89.0 3.1 fusion.64
  92.1 3.0 all-to-all-done.1
  95.1 3.2 multiply_reduce_fusion.1
  98.4 1.4 gather_fusion
  99.8 35.4 %all_to_all.53 = bf16[32,8,2048]{2,1,0:T(8,128)(2,1)S(1)} all-to-all(bf16[32,8,2048]{2,1,0:T(8,128)(2,1)S(1)} %bitcast.262), channel_id=1, replica_groups=mesh['sp_0'=8,'sp_1'=4,'tp'=8] {'sp_0','sp_1'}, dimensions={0} | all-to-all | bytes 2097152 | tf_op jit(solution)/shard_map/all_to_all | solution.py:287
  135.2 1.1 stack.2
  136.3 97.3 %all_to_all.54 = bf16[8,32,8,2048]{3,2,1,0:T(8,128)(2,1)S(1)} all-to-all(bf16[8,32,8,2048]{3,2,1,0:T(8,128)(2,1)S(1)} %stack.2), channel_id=1, replica_groups=mesh['sp_0'=8,'sp_1'=4,'tp'=8] {'tp'}, dimensions={0} | all-to-all | bytes 16777216 | tf_op jit(solution)/shard_map/all_to_all | solution.py:291
  233.6 3.2 copy-done.1
  236.9 3.8 %fusion.20 = f32[2048,256]{1,0:T(8,128)} fusion(bf16[2048,2048]{1,0:T(8,128)(2,1)S(1)} %bitcast.260, bf16[1,2048,256]{2,1,0:T(8,128)(2,1)S(1)} %copy-done.11), kind=kOutput, calls=%fused_computation.33 | convolution fusion | flops 2147483648 | bytes 11534336 | tf_op jit(solution)/shard_map/dot_general | solution.py:294
  240.6 16.8 %convolution_convert_fusion = bf16[2048,2048]{1,0:T(8,128)(2,1)} fusion(bf16[2048,2048]{1,0:T(8,128)(2,1)} %bitcast.261, f32[2048,256]{1,0:T(8,128)} %fusion.20, bf16[1,256,2048]{2,1,0:T(8,128)(2,1)S(1)} %copy-done, bf16[1,2048,256]{2,1,0:T(8,128)(2,1)} %param.42), kind=kOutput, calls=%fused_computation.3 | convolution fusion | flops 4302307328 | bytes 20971520 | tf_op jit(solution)/shard_map/dot_general | solution.py:298
  257.5 50.6 %reduce-scatter.2.cloned.1.call-done = bf16[256,2048]{1,0:T(8,128)(2,1)} async-done(((bf16[2048,2048]{1,0:T(8,128)(2,1)}), bf16[256,2048]{1,0:T(8,128)(2,1)}) %reduce-scatter.2.cloned.1.call-update) | async-done | bytes 1048592 | tf_op jit(solution)/shard_map/reduce_scatter | solution.py:297
  308.1 10.1 %all-to-all-start.4 = ((bf16[32,8,2048]{2,1,0:T(8,128)(2,1)}), bf16[32,8,2048]{2,1,0:T(8,128)(2,1)S(1)}, u32[]{:S(2)}, u32[]{:S(2)}) async-start(bf16[32,8,2048]{2,1,0:T(8,128)(2,1)} %bitcast.263), calls=%async_computation.5 | async-start | bytes 2097152 | tf_op jit(solution)/shard_map/all_to_all | solution.py:306
  318.3 0.8 constant_dynamic-slice_fusion.1
  319.2 26.5 %all-to-all-done.4 = bf16[32,8,2048]{2,1,0:T(8,128)(2,1)S(1)} async-done(((bf16[32,8,2048]{2,1,0:T(8,128)(2,1)}), bf16[32,8,2048]{2,1,0:T(8,128)(2,1)S(1)}, u32[]{:S(2)}, u32[]{:S(2)}) %all-to-all-start.4) | async-done | bytes 1048608 | tf_op jit(solution)/shard_map/all_to_all | solution.py:306
  345.7 0.9 gather_fusion.1
  347.3 1.5 multiply_reduce_fusion
  348.8 0.8 add_convert_fusion
  (134 shorter events, 12.2 us)
Async XLA Ops:
  6.5 234.1 %copy-start = (bf16[1,256,2048]{2,1,0:T(8,128)(2,1)S(1)}, bf16[1,256,2048]{2,1,0:T(8,128)(2,1)}, u32[]{:S(2)}) copy-start(bf16[1,256,2048]{2,1,0:T(8,128)(2,1)} %param.43) | copy-start | bytes 3145732
  6.5 9.4 %copy-start.6 = (bf16[512,128]{1,0:T(8,128)(2,1)S(1)}, bf16[512,128]{1,0:T(8,128)(2,1)}, u32[]{:S(2)}) copy-start(bf16[512,128]{1,0:T(8,128)(2,1)} %param.22) | copy-start | bytes 393220
  6.5 9.4 %copy-start.5 = (bf16[512,128]{1,0:T(8,128)(2,1)S(1)}, bf16[512,128]{1,0:T(8,128)(2,1)}, u32[]{:S(2)}) copy-start(bf16[512,128]{1,0:T(8,128)(2,1)} %param.23) | copy-start | bytes 393220
  13.8 3.7 %copy-start.12 = (bf16[512,128]{1,0:T(8,128)(2,1)S(1)}, bf16[512,128]{1,0:T(8,128)(2,1)}, u32[]{:S(2)}) copy-start(bf16[512,128]{1,0:T(8,128)(2,1)} %param.24) | copy-start | bytes 393220
  69.6 1.3 copy-start.3
  69.7 1.3 copy-start.9
  70.2 6.1 %copy-start.8 = (f32[2]{0:T(128)S(1)}, f32[2]{0:T(128)}, u32[]{:S(2)}) copy-start(f32[2]{0:T(128)} %param.31) | copy-start | bytes 28
  71.8 12.4 %all-to-all-start = ((bf16[8,64,128]{2,1,0:T(8,128)(2,1)}), bf16[8,64,128]{2,1,0:T(8,128)(2,1)S(1)}, u32[]{:S(2)}, u32[]{:S(2)}) async-start(bf16[8,64,128]{2,1,0:T(8,128)(2,1)} %bitcast.66), calls=%async_computation | async-start | bytes 262144 | tf_op jit(solution)/shard_map/all_to_all | solution.py:268
  79.8 3.6 %copy-start.4 = (bf16[512,128]{1,0:T(8,128)(2,1)S(1)}, bf16[512,128]{1,0:T(8,128)(2,1)}, u32[]{:S(2)}) copy-start(bf16[512,128]{1,0:T(8,128)(2,1)} %param.29) | copy-start | bytes 393220
  79.8 3.6 %copy-start.10 = (f32[128]{0:T(128)S(1)}, f32[128]{0:T(128)}, u32[]{:S(2)}) copy-start(f32[128]{0:T(128)} %param.33) | copy-start | bytes 1540
  84.2 10.9 %all-to-all-start.1 = ((bf16[8,64,128]{2,1,0:T(8,128)(2,1)}), bf16[8,64,128]{2,1,0:T(8,128)(2,1)S(1)}, u32[]{:S(2)}, u32[]{:S(2)}) async-start(bf16[8,64,128]{2,1,0:T(8,128)(2,1)} %bitcast.82), calls=%async_computation.1 | async-start | bytes 262144 | tf_op jit(solution)/shard_map/all_to_all | solution.py:269
  89.0 6.1 %copy-start.2 = (bf16[64,2048]{1,0:T(8,128)(2,1)S(1)}, bf16[64,2048]{1,0:T(8,128)(2,1)}, u32[]{:S(2)}) copy-start(bf16[64,2048]{1,0:T(8,128)(2,1)} %param.37) | copy-start | bytes 786436
  89.0 219.1 %reduce-scatter.2.cloned.1.call-start = ((), (), s32[]{:S(2)}) async-start(), calls=%async_computation.6 | async-start | bytes 9437184 | tf_op jit(solution)/shard_map/reduce_scatter | solution.py:297
  92.1 6.2 %copy-start.7 = (f32[2048]{0:T(1024)S(1)}, f32[2048]{0:T(1024)}, u32[]{:S(2)}) copy-start(f32[2048]{0:T(1024)} %param.38) | copy-start | bytes 24580
  136.3 100.6 %copy-start.11 = (bf16[1,2048,256]{2,1,0:T(8,128)(2,1)S(1)}, bf16[1,2048,256]{2,1,0:T(8,128)(2,1)}, u32[]{:S(2)}) copy-start(bf16[1,2048,256]{2,1,0:T(8,128)(2,1)} %param.41) | copy-start | bytes 3145732
  233.6 3.2 copy-start.1
  308.1 37.6 %all-to-all-start.4 = ((bf16[32,8,2048]{2,1,0:T(8,128)(2,1)}), bf16[32,8,2048]{2,1,0:T(8,128)(2,1)S(1)}, u32[]{:S(2)}, u32[]{:S(2)}) async-start(bf16[32,8,2048]{2,1,0:T(8,128)(2,1)} %bitcast.263), calls=%async_computation.5 | async-start | bytes 2097152 | tf_op jit(solution)/shard_map/all_to_all | solution.py:306
Sparse Core Ops, SparseCore 0:
  257.6 50.4 reduce-scatter.1
